TPU v7x, 32 devices: a whole 2x2x4 slice. The times are simulated.
32 devices in a mesh: ep: 8 (over z, y), tp: 4 (over x, core).
Axes of the slice: x: 2, y: 2, z: 4, core: 2. Of those that a mesh axis runs over, the one named last changes fastest.
Arguments:
- queries: bfloat16 [1024, 512], P('ep', 'tp'), may hold values from -8 to 8
- key_cache: bfloat16 [4, 64, 1024], P('tp', None, 'ep'), may hold values from -4.5 to 4.5
- value_cache: bfloat16 [4, 64, 1024], P('tp', None, 'ep'), may hold values from -6 to 6
- cum_gate: float32 [4, 1024], P('tp'), may hold values from -256 to 0, as said below
- out_weight: bfloat16 [512, 2048], replicated, may hold values from -1 to 1
- routed_input: bfloat16 [2048, 2048], P('ep'), may hold values from -6 to 6
- norm_gain: bfloat16 [2048], replicated, may hold values from 0.099609375 to 1.8984375
- routes: int32 [2048, 2], P('ep'), may hold values from 0 to 7, all different within a row; in each aligned block of 64 rows (0 to 63, 64 to 127, ...) at most 24 rows name the same one
- route_weight: float32 [2048, 2], P('ep'), may hold values from 0.2 to 1
- expert_gate: bfloat16 [8, 2048, 1024], P('ep', None, 'tp'), may hold values from -0.125 to 0.125
- expert_up: bfloat16 [8, 2048, 1024], P('ep', None, 'tp'), may hold values from -0.125 to 0.125
- expert_down: bfloat16 [8, 1024, 2048], P('ep', 'tp'), may hold values from -0.1875 to 0.1875
Outputs:
- mixed_out: bfloat16 [1024, 2048], P(('ep', 'tp'))
- expert_out: bfloat16 [2048, 2048], P(('ep', 'tp'))
Inputs may be any that keep to these rules, and one draw needn't show every extreme that they name: `cum_gate`: Non-increasing along positions in every head. `routes`: each row names 2 different experts. In each aligned block of 64 rows (the rows of one device) no expert is named by more than 24 rows, a bound that some block reaches.
All inputs are finite; a program needn't handle non-finite values.
Results may differ from a plain program's by a relative error of at most 0.012.
Values may be sent and summed in bfloat16 or wider, within the bound.
A program may use at most 64 MiB of HBM per device.

v0:
```python
import jax
import jax.numpy as jnp
from jax import lax
from jax.sharding import PartitionSpec as P


def slot_chooser(route_rows, expert_count, capacity):
    token_rows, top_count = route_rows.shape
    flat = route_rows.reshape(token_rows * top_count)
    same = (flat[:, None] == jnp.arange(expert_count, dtype=jnp.int32)[None, :]).astype(jnp.int32)
    earlier = jnp.cumsum(same, axis=0) - same
    rank = jnp.sum(earlier * same, axis=1)
    slot = flat * capacity + rank
    chosen = slot[:, None] == jnp.arange(expert_count * capacity, dtype=jnp.int32)[None, :]
    return chosen.astype(jnp.bfloat16).reshape(token_rows, top_count, expert_count * capacity)


def rms_rows(source, norm_gain):
    widened = source.astype(jnp.float32)
    scale = lax.rsqrt(jnp.mean(widened * widened, axis=-1, keepdims=True) + 1e-06)
    return (widened * scale * norm_gain.astype(jnp.float32)).astype(jnp.bfloat16)


def mixer_half(queries, key_cache, value_cache, cum_gate, out_weight):
    seq_rows = queries.shape[0]
    local_heads = key_cache.shape[0]
    head_size = key_cache.shape[1]
    group = queries.shape[1] // (local_heads * head_size)
    own_start = lax.axis_index("ep") * seq_rows
    query_heads = queries.reshape(seq_rows, local_heads, group, head_size)
    query_pos = own_start + jnp.arange(seq_rows, dtype=jnp.int32)
    gate_query = lax.dynamic_slice_in_dim(cum_gate, own_start, seq_rows, 1)
    gate_rows = jnp.transpose(gate_query)[:, :, None, None]
    scale = head_size ** (-0.5)
    best_start = jnp.full((seq_rows, local_heads, group), -jnp.inf, jnp.float32)
    total_start = jnp.zeros((seq_rows, local_heads, group), jnp.float32)
    summed_start = jnp.zeros((seq_rows, local_heads * group * head_size), jnp.float32)
    pieces = (
        lax.all_gather(key_cache, "ep", axis=2, tiled=True),
        lax.all_gather(value_cache, "ep", axis=2, tiled=True),
    )

    def update(state):
        best, total, summed = state
        key_piece, value_piece = pieces
        width = key_piece.shape[2]
        scores = (
            jnp.einsum("thgd,hds->thgs", query_heads, key_piece, preferred_element_type=jnp.float32)
            * scale
        )
        scores = scores + gate_rows - cum_gate[None, :, None, :]
        key_pos = jnp.arange(width, dtype=jnp.int32)
        allowed = key_pos[None, :] <= query_pos[:, None]
        scores = jnp.where(allowed[:, None, None, :], scores, -jnp.inf)
        new_best = jnp.max(scores, axis=-1)
        factor = jnp.exp(best - new_best)
        weights = jnp.exp(scores - new_best[..., None])
        new_total = total * factor + jnp.sum(weights, axis=-1)
        product = jnp.einsum(
            "thgs,hds->thgd",
            weights.astype(jnp.bfloat16),
            value_piece,
            preferred_element_type=jnp.float32,
        )
        new_summed = summed.reshape(product.shape) * factor[..., None] + product
        return (new_best, new_total, new_summed.reshape(seq_rows, local_heads * group * head_size))

    best, total, summed = lax.cond(
        jnp.int32(0) <= own_start,
        update,
        lambda state: state,
        (best_start, total_start, summed_start),
    )
    attended = summed.reshape(seq_rows, local_heads, group, head_size) / total[..., None]
    attended = attended.astype(jnp.bfloat16).reshape(seq_rows, local_heads * group * head_size)
    by_position = lax.all_to_all(attended, "tp", split_axis=0, concat_axis=1, tiled=True)
    return jnp.dot(by_position, out_weight, preferred_element_type=jnp.float32).astype(jnp.bfloat16)


def expert_half(routed_input, norm_gain, routes, route_weight, expert_gate, expert_up, expert_down):
    group_size = lax.axis_size("tp")
    ep_size = lax.axis_size("ep")
    tp_index = lax.axis_index("tp")
    seq_rows, width = routed_input.shape
    own_rows = seq_rows // group_size
    local_experts = expert_gate.shape[0]
    expert_count = local_experts * ep_size
    top_count = routes.shape[1]
    capacity = max(2, own_rows * top_count * 3 // (2 * expert_count))
    per_device = local_experts * capacity
    mine = lax.dynamic_slice_in_dim(routed_input, tp_index * own_rows, own_rows, 0)
    own_routes = lax.dynamic_slice_in_dim(routes, tp_index * own_rows, own_rows, 0)
    chooser = slot_chooser(own_routes, expert_count, capacity)
    normed = rms_rows(mine, norm_gain)
    outgoing = jnp.einsum("tks,td->sd", chooser, normed, preferred_element_type=jnp.float32).astype(
        jnp.bfloat16
    )
    arrived = lax.all_to_all(
        outgoing.reshape(1, ep_size, per_device, width),
        "ep",
        split_axis=1,
        concat_axis=1,
        tiled=True,
    )
    received = lax.all_gather(arrived, "tp", axis=0, tiled=True)
    blocks = received.shape[0]
    divide_point = received.reshape(blocks, ep_size, local_experts, capacity, width)
    gate = jnp.einsum(
        "abecd,edf->abecf", divide_point, expert_gate, preferred_element_type=jnp.float32
    )
    upper = jnp.einsum(
        "abecd,edf->abecf", divide_point, expert_up, preferred_element_type=jnp.float32
    )
    hidden = (jax.nn.silu(gate) * upper).astype(jnp.bfloat16)
    partial_value = jnp.einsum(
        "abecf,efd->abecd", hidden, expert_down, preferred_element_type=jnp.float32
    )
    rounded = lax.optimization_barrier(partial_value.astype(jnp.bfloat16)).astype(jnp.float32)
    summed = lax.psum_scatter(
        rounded.reshape(lax.axis_size("tp") * 1, ep_size, per_device, width).astype(jnp.bfloat16),
        "tp",
        scatter_dimension=0,
        tiled=True,
    )
    returned = lax.all_to_all(summed, "ep", split_axis=1, concat_axis=1, tiled=True)
    picked = jnp.einsum(
        "tks,sd->tkd",
        chooser,
        returned.reshape(ep_size * per_device, width),
        preferred_element_type=jnp.float32,
    )
    own_weight = lax.dynamic_slice_in_dim(route_weight, tp_index * own_rows, own_rows, 0)
    return jnp.sum(own_weight[:, :, None] * picked, axis=1).astype(jnp.bfloat16)


def body(
    queries,
    key_cache,
    value_cache,
    cum_gate,
    out_weight,
    routed_input,
    norm_gain,
    routes,
    route_weight,
    expert_gate,
    expert_up,
    expert_down,
):
    mixed_out = mixer_half(queries, key_cache, value_cache, cum_gate, out_weight)
    expert_out = expert_half(
        routed_input, norm_gain, routes, route_weight, expert_gate, expert_up, expert_down
    )
    return (mixed_out, expert_out)


def solution(mesh):
    return jax.shard_map(
        body,
        mesh=mesh,
        in_specs=(
            P("ep", "tp"),
            P("tp", None, "ep"),
            P("tp", None, "ep"),
            P("tp", None),
            P(),
            P("ep", None),
            P(),
            P("ep", None),
            P("ep", None),
            P("ep", None, "tp"),
            P("ep", None, "tp"),
            P("ep", "tp", None),
        ),
        out_specs=(P(("ep", "tp"), None), P(("ep", "tp"), None)),
        check_vma=False,
    )
```

profile of v0, /device:TPU:0, one launch (start us, length us, event | category | flops | bytes accessed | tf_op | source)
XLA Modules:
  0.0 172.3 jit_solution(1201821751376832034)
XLA Ops:
  7.2 0.9 constant_dynamic-slice_fusion
  8.5 0.2 reduce_window_sum.11
  8.7 0.2 select_reduce_fusion
  8.9 0.1 reduce_sum.48
  9.1 0.8 multiply_add_fusion
  9.9 1.1 fusion.23
  11.1 0.7 convert_element_type.68
  11.8 1.4 convolution_convert_fusion.1
  13.1 27.4 %all_to_all.29 = bf16[1,8,24,2048]{3,2,0,1:T(8,128)(2,1)} all-to-all(bf16[1,8,24,2048]{3,2,0,1:T(8,128)(2,1)S(1)} %bitcast.129), channel_id=1, replica_groups=mesh['ep'=8,'tp'=4] {'ep'}, dimensions={1} | all-to-all | bytes 1572864 | tf_op jit(solution)/shard_map/all_to_all | solution.py:98
  40.6 27.6 %all-gather.2.cloned.1.call-done = bf16[4,8,24,2048]{3,2,1,0:T(8,128)(2,1)} async-done(((bf16[1,8,24,2048]{3,2,1,0:T(8,128)(2,1)}), bf16[4,8,24,2048]{3,2,1,0:T(8,128)(2,1)}) %all-gather.2.cloned.1.call-update) | async-done | bytes 3145744 | tf_op jit(solution)/shard_map/all_gather | solution.py:105
  68.2 3.8 %convolution_bitcast_fusion.2 = f32[4,8,1,24,256]{4,3,1,0,2:T(8,128)} fusion(bf16[4,8,24,2048]{3,2,1,0:T(8,128)(2,1)} %all-gather.2.cloned.1.call-done, bf16[1,2048,256]{2,1,0:T(8,128)(2,1)S(1)} %copy-done.5), kind=kOutput, calls=%fused_computation.26 | convolution fusion | flops 805306368 | bytes 4980736 | tf_op jit(solution)/shard_map/abecd,edf->abecf/dot_general | solution.py:108
  72.0 7.9 %fusion.13 = bf16[4,8,1,24,2048]{4,3,1,0,2:T(8,128)(2,1)} fusion(bf16[1,256,2048]{2,1,0:T(8,128)(2,1)} %param.25, bf16[4,8,24,2048]{3,2,1,0:T(8,128)(2,1)} %all-gather.2.cloned.1.call-done, bf16[1,2048,256]{2,1,0:T(8,128)(2,1)} %param.24, f32[4,8,1,24,256]{4,3,1,0,2:T(8,128)} %convolution_bitcast_fusion.2), kind=kOutput, calls=%fused_computation.21 | convolution fusion | flops 1613365248 | bytes 9175040 | tf_op jit(solution)/shard_map/abecf,efd->abecd/dot_general | solution.py:115
  79.9 0.7 copy-done.2
  80.6 26.2 %all_gather.10 = bf16[1,64,1024]{2,1,0:T(8,128)(2,1)S(1)} all-gather(bf16[1,64,128]{2,1,0:T(8,128)(2,1)S(1)} %copy-done.2), channel_id=1, replica_groups=mesh['ep'=8,'tp'=4] {'ep'}, dimensions={2}, use_global_device_ids=true | all-gather | bytes 147456 | tf_op jit(solution)/shard_map/all_gather | solution.py:40
  106.7 26.2 %all_gather.9 = bf16[1,64,1024]{2,1,0:T(8,128)(2,1)S(1)} all-gather(bf16[1,64,128]{2,1,0:T(8,128)(2,1)S(1)} %copy-done.3), channel_id=1, replica_groups=mesh['ep'=8,'tp'=4] {'ep'}, dimensions={2}, use_global_device_ids=true | all-gather | bytes 147456 | tf_op jit(solution)/shard_map/all_gather | solution.py:39
  132.9 1.2 conditional.1
  133.2 0.4 fusion.41
  133.7 0.2 fusion.7
  133.8 0.3 fusion.5
  134.3 6.3 %all_to_all.30 = bf16[4,32,128]{2,1,0:T(8,128)(2,1)S(1)} all-to-all(bf16[4,32,128]{2,1,0:T(8,128)(2,1)S(1)} %bitcast.133), channel_id=1, replica_groups=mesh['ep'=8,'tp'=4] {'tp'}, dimensions={0} | all-to-all | bytes 65536 | tf_op jit(solution)/shard_map/all_to_all | solution.py:76
  140.6 3.5 %all-to-all-start.2 = ((bf16[1,8,24,2048]{3,2,0,1:T(8,128)(2,1)}), bf16[1,8,24,2048]{3,2,0,1:T(8,128)(2,1)S(1)}, u32[]{:S(2)}, u32[]{:S(2)}) async-start(bf16[1,8,24,2048]{3,2,0,1:T(8,128)(2,1)} %bitcast.130), calls=%async_computation.3 | async-start | bytes 1572864 | tf_op jit(solution)/shard_map/all_to_all | solution.py:125
  144.2 1.1 convolution_convert_fusion.2
  145.4 19.1 %all-to-all-done.2 = bf16[1,8,24,2048]{3,2,0,1:T(8,128)(2,1)S(1)} async-done(((bf16[1,8,24,2048]{3,2,0,1:T(8,128)(2,1)}), bf16[1,8,24,2048]{3,2,0,1:T(8,128)(2,1)S(1)}, u32[]{:S(2)}, u32[]{:S(2)}) %all-to-all-start.2) | async-done | bytes 786464 | tf_op jit(solution)/shard_map/all_to_all | solution.py:125
  164.4 1.1 fusion.15
  (33 shorter events, 1.1 us)
Async XLA Ops:
  7.2 137.1 %copy-start = (bf16[512,2048]{1,0:T(8,128)(2,1)S(1)}, bf16[512,2048]{1,0:T(8,128)(2,1)}, u32[]{:S(2)}) copy-start(bf16[512,2048]{1,0:T(8,128)(2,1)} %param.18) | copy-start | bytes 6291460
  7.2 61.0 %copy-start.5 = (bf16[1,2048,256]{2,1,0:T(8,128)(2,1)S(1)}, bf16[1,2048,256]{2,1,0:T(8,128)(2,1)}, u32[]{:S(2)}) copy-start(bf16[1,2048,256]{2,1,0:T(8,128)(2,1)} %param.23) | copy-start | bytes 3145732
  7.2 61.0 %all-gather.2.cloned.1.call-start = ((), (), s32[]{:S(2)}) async-start(), calls=%async_computation.4 | async-start | bytes 3932160 | tf_op jit(solution)/shard_map/all_gather | solution.py:105
  40.5 100.0 %reduce-scatter.2.cloned.1.call-start = ((), (), s32[]{:S(2)}) async-start(), calls=%async_computation.5 | async-start | bytes 3932160 | tf_op jit(solution)/shard_map/reduce_scatter | solution.py:119
  79.8 0.7 copy-start.2
  79.8 26.9 %copy-start.3 = (bf16[1,64,128]{2,1,0:T(8,128)(2,1)S(1)}, bf16[1,64,128]{2,1,0:T(8,128)(2,1)}, u32[]{:S(2)}) copy-start(bf16[1,64,128]{2,1,0:T(8,128)(2,1)} %param.15) | copy-start | bytes 49156
  79.8 53.1 %copy-start.1 = (bf16[128,128]{1,0:T(8,128)(2,1)S(1)}, bf16[128,128]{1,0:T(8,128)(2,1)}, u32[]{:S(2)}) copy-start(bf16[128,128]{1,0:T(8,128)(2,1)} %param.14) | copy-start | bytes 98308
  79.8 53.1 %copy-start.6 = (f32[1,1024]{1,0:T(1,128)S(1)}, f32[1,1024]{1,0:T(1,128)}, u32[]{:S(2)}) copy-start(f32[1,1024]{1,0:T(1,128)} %param.17) | copy-start | bytes 12292
  132.9 11.2 %copy-start.4 = (f32[256,2]{0,1:T(2,128)S(1)}, f32[256,2]{0,1:T(2,128)}, u32[]{:S(2)}) copy-start(f32[256,2]{0,1:T(2,128)} %param.22) | copy-start | bytes 6148
  140.6 23.8 %all-to-all-start.2 = ((bf16[1,8,24,2048]{3,2,0,1:T(8,128)(2,1)}), bf16[1,8,24,2048]{3,2,0,1:T(8,128)(2,1)S(1)}, u32[]{:S(2)}, u32[]{:S(2)}) async-start(bf16[1,8,24,2048]{3,2,0,1:T(8,128)(2,1)} %bitcast.130), calls=%async_computation.3 | async-start | bytes 1572864 | tf_op jit(solution)/shard_map/all_to_all | solution.py:125
Sparse Core Ops, SparseCore 0:
  40.6 27.5 all-gather.1
  80.0 37.8 reduce-scatter.1
where the time goes:
time: 173 us; the launch traced here: 172 us
  blocking collectives  86 us (50%)
  waiting for transfers between devices  46.7 us (27%)
  matrix products  15.9 us (9%)
  between operations  14.2 us (8%)
  starting transfers between devices  3.63 us (2%)
  other arithmetic  3.38 us (2%)
  local copies, waits for them, and re-layouts  2.47 us (1%)
    all_gather x1, waiting for transfers between devices, expert_half(): received = lax.all_gather(arrived, 'tp', axis=0, tiled=True)  27.6 us
    all_to_all x1, blocking collectives, expert_half(): lax.all_to_all(outgoing.reshape(1, ep_size, per_device, width), 'ep', spl...  27.4 us
    all_gather x1, blocking collectives, mixer_half(): lax.all_gather(value_cache, 'ep', axis=2, tiled=True)  26.2 us
    all_gather x1, blocking collectives, mixer_half(): lax.all_gather(key_cache, 'ep', axis=2, tiled=True)  26.2 us
    all_to_all x1, waiting for transfers between devices, expert_half(): lax.all_to_all(summed, 'ep', split_axis=1, concat_axis=1, tiled=True)  19.1 us
    dot_general x1, matrix products, expert_half(): jnp.einsum('abecf,efd->abecd', hidden, expert_down, preferred_element_typ...  7.85 us
    all_to_all x1, blocking collectives, mixer_half(): lax.all_to_all(attended, 'tp', split_axis=0, concat_axis=1, tiled=True)  6.3 us
    dot_general x1, matrix products, expert_half(): jnp.einsum('abecd,edf->abecf', divide_point, expert_gate, preferred_eleme...  3.78 us
  transfers between devices with their start and end apart: 3, of which 2 were waited for; matrix products, arithmetic and copies ran while one was open for 1% of the time, Pallas kernels for 0%

commit v1 on v0

--- a/solution.py
+++ b/solution.py
@@ -95,13 +95,19 @@
     outgoing = jnp.einsum("tks,td->sd", chooser, normed, preferred_element_type=jnp.float32).astype(
         jnp.bfloat16
     )
-    arrived = lax.all_to_all(
-        outgoing.reshape(1, ep_size, per_device, width),
-        "ep",
-        split_axis=1,
-        concat_axis=1,
-        tiled=True,
-    )
+    shard = outgoing.reshape(1, ep_size, per_device, width)
+    ways, here = (lax.axis_size("ep"), lax.axis_index("ep"))
+    width_2 = shard.shape[1] // ways
+    shape = list(shard.shape)
+    shape[1] = width_2
+    height = shape[1]
+    shape[1] = height * ways
+    arrived = jnp.zeros(shape, shard.dtype)
+    for mask in range(ways):
+        part = lax.dynamic_slice_in_dim(shard, (here ^ mask) * width_2, width_2, axis=1)
+        if mask:
+            part = lax.ppermute(part, "ep", [(d, d ^ mask) for d in range(ways)])
+        arrived = lax.dynamic_update_slice_in_dim(arrived, part, (here ^ mask) * height, axis=1)
     received = lax.all_gather(arrived, "tp", axis=0, tiled=True)
     blocks = received.shape[0]
     divide_point = received.reshape(blocks, ep_size, local_experts, capacity, width)

time: 173 us -> 172 us (level)
  blocking collectives: 86 us -> 58.6 us
  waiting for transfers between devices: 46.7 us -> 59.6 us
  starting transfers between devices: 3.63 us -> 16.2 us
    all_to_all x1 -> x0, blocking collectives: 27.4 us -> none  [expert_half(): lax.all_to_all(outgoing.reshape(1, ep_size, per_device, width), 'ep', spl...]
    ppermute x0 -> x7, starting transfers between devices: none -> 12.6 us  [expert_half(): part = lax.ppermute(part, 'ep', [(d, d ^ mask) for d in range(ways)])]
    ppermute x0 -> x7, waiting for transfers between devices: none -> 10.1 us  [expert_half(): part = lax.ppermute(part, 'ep', [(d, d ^ mask) for d in range(ways)])]
    all_gather x1, waiting for transfers between devices: 27.6 us -> 30.4 us  [expert_half(): received = lax.all_gather(arrived, 'tp', axis=0, tiled=True)]
  transfers between devices with their start and end apart: 3 -> 10, of which waited for: 2 -> 3; matrix products, arithmetic and copies ran while one was open for 1% -> 2% of each run, Pallas kernels for 0% -> 0%
where the time goes in v1:
time: 172 us
  waiting for transfers between devices  59.6 us (35%)
  blocking collectives  58.6 us (34%)
  starting transfers between devices  16.2 us (9%)
  matrix products  15.8 us (9%)
  between operations  14.3 us (8%)
  local copies, waits for them, and re-layouts  3.55 us (2%)
  other arithmetic  3.38 us (2%)
    all_gather x1, waiting for transfers between devices, expert_half(): received = lax.all_gather(arrived, 'tp', axis=0, tiled=True)  30.4 us
    all_gather x1, blocking collectives, mixer_half(): lax.all_gather(value_cache, 'ep', axis=2, tiled=True)  26.2 us
    all_gather x1, blocking collectives, mixer_half(): lax.all_gather(key_cache, 'ep', axis=2, tiled=True)  26.2 us
    all_to_all x1, waiting for transfers between devices, expert_half(): lax.all_to_all(summed, 'ep', split_axis=1, concat_axis=1, tiled=True)  19.1 us
    ppermute x7, starting transfers between devices, expert_half(): part = lax.ppermute(part, 'ep', [(d, d ^ mask) for d in range(ways)])  12.6 us
    ppermute x7, waiting for transfers between devices, expert_half(): part = lax.ppermute(part, 'ep', [(d, d ^ mask) for d in range(ways)])  10.1 us
    dot_general x1, matrix products, expert_half(): jnp.einsum('abecf,efd->abecd', hidden, expert_down, preferred_element_typ...  7.52 us
    all_to_all x1, blocking collectives, mixer_half(): lax.all_to_all(attended, 'tp', split_axis=0, concat_axis=1, tiled=True)  6.3 us
  transfers between devices with their start and end apart: 10, of which 3 were waited for; matrix products, arithmetic and copies ran while one was open for 2% of the time, Pallas kernels for 0%

profile of v1, /device:TPU:0, one launch (start us, length us, event | category | flops | bytes accessed | tf_op | source)
XLA Modules:
  0.0 171.6 jit_solution(7453408059214138154)
XLA Ops:
  7.3 0.9 constant_dynamic-slice_fusion.7
  9.1 0.8 multiply_add_fusion
  9.9 1.1 fusion.18
  11.0 0.7 convert_element_type.68
  11.7 1.4 convolution_convert_fusion.1
  13.3 3.1 %collective-permute-start = (bf16[1,1,24,2048]{3,2,1,0:T(8,128)(2,1)S(1)}, bf16[1,1,24,2048]{3,2,1,0:T(8,128)(2,1)S(1)}, u32[]{:S(2)}, u32[]{:S(2)}) collective-permute-start(bf16[1,1,24,2048]{3,2,1,0:T(8,128)(2,1)S(1)} %get-tuple-element.111), channel_id=1, source_target_pairs={{0,4},{4,0},{8,12},{12,8},{16,20},{20,16},{24,28},{28,24},{1,5},{5... | collective-permute-start | bytes 294920 | tf_op jit(solution)/shard_map/ppermute | solution.py:109
  16.4 1.6 collective-permute-start.1
  17.9 3.0 %collective-permute-start.3 = (bf16[1,1,24,2048]{3,2,1,0:T(8,128)(2,1)S(1)}, bf16[1,1,24,2048]{3,2,1,0:T(8,128)(2,1)S(1)}, u32[]{:S(2)}, u32[]{:S(2)}) collective-permute-start(bf16[1,1,24,2048]{3,2,1,0:T(8,128)(2,1)S(1)} %get-tuple-element.108), channel_id=1, source_target_pairs={{0,16},{4,20},{8,24},{12,28},{16,0},{20,4},{24,8},{28,12},{1,17},{... | collective-permute-start | bytes 294920 | tf_op jit(solution)/shard_map/ppermute | solution.py:109
  20.9 1.3 collective-permute-start.4
  22.2 3.6 %collective-permute-start.5 = (bf16[1,1,24,2048]{3,2,1,0:T(8,128)(2,1)S(1)}, bf16[1,1,24,2048]{3,2,1,0:T(8,128)(2,1)S(1)}, u32[]{:S(2)}, u32[]{:S(2)}) collective-permute-start(bf16[1,1,24,2048]{3,2,1,0:T(8,128)(2,1)S(1)} %get-tuple-element.106), channel_id=1, source_target_pairs={{0,24},{4,28},{8,16},{12,20},{16,8},{20,12},{24,0},{28,4},{1,25},{... | collective-permute-start | bytes 294920 | tf_op jit(solution)/shard_map/ppermute | solution.py:109
  26.0 10.1 %collective-permute-done.4 = bf16[1,1,24,2048]{3,2,1,0:T(8,128)(2,1)S(1)} collective-permute-done((bf16[1,1,24,2048]{3,2,1,0:T(8,128)(2,1)S(1)}, bf16[1,1,24,2048]{3,2,1,0:T(8,128)(2,1)S(1)}, u32[]{:S(2)}, u32[]{:S(2)}) %collective-permute-start.4) | collective-permute-done | bytes 98336 | tf_op jit(solution)/shard_map/ppermute | solution.py:109
  36.2 0.9 copy-done.1
  37.2 30.4 %all-gather.2.cloned.1.call-done = bf16[4,8,24,2048]{3,2,1,0:T(8,128)(2,1)} async-done(((bf16[1,8,24,2048]{3,2,1,0:T(8,128)(2,1)}), bf16[4,8,24,2048]{3,2,1,0:T(8,128)(2,1)}) %all-gather.2.cloned.1.call-update) | async-done | bytes 3145744 | tf_op jit(solution)/shard_map/all_gather | solution.py:111
  67.5 4.0 %convolution_bitcast_fusion.1 = f32[4,8,1,24,256]{4,3,1,0,2:T(8,128)} fusion(bf16[4,8,24,2048]{3,2,1,0:T(8,128)(2,1)} %all-gather.2.cloned.1.call-done, bf16[1,2048,256]{2,1,0:T(8,128)(2,1)} %param.24), kind=kOutput, calls=%fused_computation.25 | convolution fusion | flops 805306368 | bytes 4980736 | tf_op jit(solution)/shard_map/abecd,edf->abecf/dot_general | solution.py:117
  71.6 7.5 %fusion.13 = bf16[4,8,1,24,2048]{4,3,1,0,2:T(8,128)(2,1)} fusion(bf16[1,256,2048]{2,1,0:T(8,128)(2,1)S(1)} %copy-done.6, f32[4,8,1,24,256]{4,3,1,0,2:T(8,128)} %convolution_bitcast_fusion.1, bf16[4,8,24,2048]{3,2,1,0:T(8,128)(2,1)} %all-gather.2.cloned.1.call-done, bf16[1,2048,256]{2,1,0:T(8,128)(2,1)} %param.23), kind=kOutput, calls=%fused_computation.21 | convolution fusion | flops 1613365248 | bytes 9175040 | tf_op jit(solution)/shard_map/abecf,efd->abecd/dot_general | solution.py:121
  79.1 0.7 copy-done.3
  79.8 26.2 %all_gather.10 = bf16[1,64,1024]{2,1,0:T(8,128)(2,1)S(1)} all-gather(bf16[1,64,128]{2,1,0:T(8,128)(2,1)S(1)} %copy-done.3), channel_id=1, replica_groups=mesh['ep'=8,'tp'=4] {'ep'}, dimensions={2}, use_global_device_ids=true | all-gather | bytes 147456 | tf_op jit(solution)/shard_map/all_gather | solution.py:40
  106.0 26.2 %all_gather.9 = bf16[1,64,1024]{2,1,0:T(8,128)(2,1)S(1)} all-gather(bf16[1,64,128]{2,1,0:T(8,128)(2,1)S(1)} %copy-done.4), channel_id=1, replica_groups=mesh['ep'=8,'tp'=4] {'ep'}, dimensions={2}, use_global_device_ids=true | all-gather | bytes 147456 | tf_op jit(solution)/shard_map/all_gather | solution.py:39
  132.2 1.2 conditional.1
  133.5 6.3 %all_to_all.24 = bf16[4,32,128]{2,1,0:T(8,128)(2,1)S(1)} all-to-all(bf16[4,32,128]{2,1,0:T(8,128)(2,1)S(1)} %bitcast.126), channel_id=1, replica_groups=mesh['ep'=8,'tp'=4] {'tp'}, dimensions={0} | all-to-all | bytes 65536 | tf_op jit(solution)/shard_map/all_to_all | solution.py:76
  139.8 3.5 %all-to-all-start.1 = ((bf16[1,8,24,2048]{3,2,0,1:T(8,128)(2,1)}), bf16[1,8,24,2048]{3,2,0,1:T(8,128)(2,1)S(1)}, u32[]{:S(2)}, u32[]{:S(2)}) async-start(bf16[1,8,24,2048]{3,2,0,1:T(8,128)(2,1)} %bitcast.123), calls=%async_computation.2 | async-start | bytes 1572864 | tf_op jit(solution)/shard_map/all_to_all | solution.py:131
  143.5 1.1 convolution_convert_fusion.2
  144.6 19.1 %all-to-all-done.1 = bf16[1,8,24,2048]{3,2,0,1:T(8,128)(2,1)S(1)} async-done(((bf16[1,8,24,2048]{3,2,0,1:T(8,128)(2,1)}), bf16[1,8,24,2048]{3,2,0,1:T(8,128)(2,1)S(1)}, u32[]{:S(2)}, u32[]{:S(2)}) %all-to-all-start.1) | async-done | bytes 786464 | tf_op jit(solution)/shard_map/all_to_all | solution.py:131
  163.7 1.1 fusion.14
  (57 shorter events, 2.8 us)
Async XLA Ops:
  7.2 136.3 %copy-start = (bf16[512,2048]{1,0:T(8,128)(2,1)S(1)}, bf16[512,2048]{1,0:T(8,128)(2,1)}, u32[]{:S(2)}) copy-start(bf16[512,2048]{1,0:T(8,128)(2,1)} %param.18) | copy-start | bytes 6291460
  7.2 60.4 %all-gather.2.cloned.1.call-start = ((), (), s32[]{:S(2)}) async-start(), calls=%async_computation.3 | async-start | bytes 3932160 | tf_op jit(solution)/shard_map/all_gather | solution.py:111
  13.3 8.9 %collective-permute-start = (bf16[1,1,24,2048]{3,2,1,0:T(8,128)(2,1)S(1)}, bf16[1,1,24,2048]{3,2,1,0:T(8,128)(2,1)S(1)}, u32[]{:S(2)}, u32[]{:S(2)}) collective-permute-start(bf16[1,1,24,2048]{3,2,1,0:T(8,128)(2,1)S(1)} %get-tuple-element.111), channel_id=1, source_target_pairs={{0,4},{4,0},{8,12},{12,8},{16,20},{20,16},{24,28},{28,24},{1,5},{5... | collective-permute-start | bytes 294920 | tf_op jit(solution)/shard_map/ppermute | solution.py:109
  16.4 9.5 %collective-permute-start.1 = (bf16[1,1,24,2048]{3,2,1,0:T(8,128)(2,1)S(1)}, bf16[1,1,24,2048]{3,2,1,0:T(8,128)(2,1)S(1)}, u32[]{:S(2)}, u32[]{:S(2)}) collective-permute-start(bf16[1,1,24,2048]{3,2,1,0:T(8,128)(2,1)S(1)} %get-tuple-element.110), channel_id=1, source_target_pairs={{0,8},{4,12},{8,0},{12,4},{16,24},{20,28},{24,16},{28,20},{1,9},{5... | collective-permute-start | bytes 294920 | tf_op jit(solution)/shard_map/ppermute | solution.py:109
  17.9 8.0 %collective-permute-start.2 = (bf16[1,1,24,2048]{3,2,1,0:T(8,128)(2,1)S(1)}, bf16[1,1,24,2048]{3,2,1,0:T(8,128)(2,1)S(1)}, u32[]{:S(2)}, u32[]{:S(2)}) collective-permute-start(bf16[1,1,24,2048]{3,2,1,0:T(8,128)(2,1)S(1)} %get-tuple-element.109), channel_id=1, source_target_pairs={{0,12},{4,8},{8,4},{12,0},{16,28},{20,24},{24,20},{28,16},{1,13},{... | collective-permute-start | bytes 294920 | tf_op jit(solution)/shard_map/ppermute | solution.py:109
  17.9 8.0 %collective-permute-start.3 = (bf16[1,1,24,2048]{3,2,1,0:T(8,128)(2,1)S(1)}, bf16[1,1,24,2048]{3,2,1,0:T(8,128)(2,1)S(1)}, u32[]{:S(2)}, u32[]{:S(2)}) collective-permute-start(bf16[1,1,24,2048]{3,2,1,0:T(8,128)(2,1)S(1)} %get-tuple-element.108), channel_id=1, source_target_pairs={{0,16},{4,20},{8,24},{12,28},{16,0},{20,4},{24,8},{28,12},{1,17},{... | collective-permute-start | bytes 294920 | tf_op jit(solution)/shard_map/ppermute | solution.py:109
  20.9 15.2 %collective-permute-start.4 = (bf16[1,1,24,2048]{3,2,1,0:T(8,128)(2,1)S(1)}, bf16[1,1,24,2048]{3,2,1,0:T(8,128)(2,1)S(1)}, u32[]{:S(2)}, u32[]{:S(2)}) collective-permute-start(bf16[1,1,24,2048]{3,2,1,0:T(8,128)(2,1)S(1)} %get-tuple-element.107), channel_id=1, source_target_pairs={{0,20},{4,16},{8,28},{12,24},{16,4},{20,0},{24,12},{28,8},{1,21},{... | collective-permute-start | bytes 294920 | tf_op jit(solution)/shard_map/ppermute | solution.py:109
  22.2 13.9 %collective-permute-start.5 = (bf16[1,1,24,2048]{3,2,1,0:T(8,128)(2,1)S(1)}, bf16[1,1,24,2048]{3,2,1,0:T(8,128)(2,1)S(1)}, u32[]{:S(2)}, u32[]{:S(2)}) collective-permute-start(bf16[1,1,24,2048]{3,2,1,0:T(8,128)(2,1)S(1)} %get-tuple-element.106), channel_id=1, source_target_pairs={{0,24},{4,28},{8,16},{12,20},{16,8},{20,12},{24,0},{28,4},{1,25},{... | collective-permute-start | bytes 294920 | tf_op jit(solution)/shard_map/ppermute | solution.py:109
  25.8 10.3 %collective-permute-start.6 = (bf16[1,1,24,2048]{3,2,1,0:T(8,128)(2,1)S(1)}, bf16[1,1,24,2048]{3,2,1,0:T(8,128)(2,1)S(1)}, u32[]{:S(2)}, u32[]{:S(2)}) collective-permute-start(bf16[1,1,24,2048]{3,2,1,0:T(8,128)(2,1)S(1)} %get-tuple-element.105), channel_id=1, source_target_pairs={{0,28},{4,24},{8,20},{12,16},{16,12},{20,8},{24,4},{28,0},{1,29},{... | collective-permute-start | bytes 294920 | tf_op jit(solution)/shard_map/ppermute | solution.py:109
  36.2 0.9 copy-start.1
  37.1 34.5 %copy-start.6 = (bf16[1,256,2048]{2,1,0:T(8,128)(2,1)S(1)}, bf16[1,256,2048]{2,1,0:T(8,128)(2,1)}, u32[]{:S(2)}) copy-start(bf16[1,256,2048]{2,1,0:T(8,128)(2,1)} %param.25) | copy-start | bytes 3145732
  37.1 102.7 %reduce-scatter.2.cloned.1.call-start = ((), (), s32[]{:S(2)}) async-start(), calls=%async_computation.4 | async-start | bytes 3932160 | tf_op jit(solution)/shard_map/reduce_scatter | solution.py:125
  79.1 0.7 copy-start.3
  79.1 26.9 %copy-start.4 = (bf16[1,64,128]{2,1,0:T(8,128)(2,1)S(1)}, bf16[1,64,128]{2,1,0:T(8,128)(2,1)}, u32[]{:S(2)}) copy-start(bf16[1,64,128]{2,1,0:T(8,128)(2,1)} %param.15) | copy-start | bytes 49156
  79.1 53.1 %copy-start.2 = (bf16[128,128]{1,0:T(8,128)(2,1)S(1)}, bf16[128,128]{1,0:T(8,128)(2,1)}, u32[]{:S(2)}) copy-start(bf16[128,128]{1,0:T(8,128)(2,1)} %param.14) | copy-start | bytes 98308
  79.1 53.1 %copy-start.7 = (f32[1,1024]{1,0:T(1,128)S(1)}, f32[1,1024]{1,0:T(1,128)}, u32[]{:S(2)}) copy-start(f32[1,1024]{1,0:T(1,128)} %param.17) | copy-start | bytes 12292
  132.2 11.2 %copy-start.5 = (f32[256,2]{0,1:T(2,128)S(1)}, f32[256,2]{0,1:T(2,128)}, u32[]{:S(2)}) copy-start(f32[256,2]{0,1:T(2,128)} %param.22) | copy-start | bytes 6148
  139.8 23.8 %all-to-all-start.1 = ((bf16[1,8,24,2048]{3,2,0,1:T(8,128)(2,1)}), bf16[1,8,24,2048]{3,2,0,1:T(8,128)(2,1)S(1)}, u32[]{:S(2)}, u32[]{:S(2)}) async-start(bf16[1,8,24,2048]{3,2,0,1:T(8,128)(2,1)} %bitcast.123), calls=%async_computation.2 | async-start | bytes 1572864 | tf_op jit(solution)/shard_map/all_to_all | solution.py:131
Sparse Core Ops, SparseCore 0:
  37.2 30.2 all-gather.1
  79.2 37.8 reduce-scatter.1
